TPU v7x, 32 devices: a whole 2x2x4 slice. The times are simulated.
32 devices in a mesh: gr: 2 (over x), sp: 8 (over z, y), tp: 2 (over core).
Axes of the slice: x: 2, y: 2, z: 4, core: 2. Of those that a mesh axis runs over, the one named last changes fastest.
Arguments:
- tokens: bfloat16 [2, 2, 6144, 2048], P('gr', 'tp', 'sp'), may hold values from -6 to 6
- key_weight: bfloat16 [2048, 2048], replicated, may hold values from -0.125 to 0.125
- value_weight: bfloat16 [2048, 2048], replicated, may hold values from -0.125 to 0.125
- cum_gate: float32 [2, 32, 2, 6144], P('gr', None, 'tp', 'sp'), may hold values from -12588 to 0, as said below
- query: bfloat16 [2, 32, 64], P('gr', 'sp'), may hold values from -12 to 12
Outputs:
- kv_cache: bfloat16 [2, 32, 12288, 128], P('gr', 'sp', 'tp')
- gate_cache: float32 [2, 32, 12288], P('gr', 'sp', 'tp')
- read: bfloat16 [2, 32, 64], P('gr', 'sp')
Inputs may be any that keep to these rules, and one draw needn't show every extreme that they name: `cum_gate`: each head's entries never rise along the positions.
All inputs are finite; a program needn't handle non-finite values.
Results may differ from a plain program's by a relative error of at most 0.012.
Values may be sent and summed in bfloat16 or wider, within the bound.
A program may use at most 128 MiB of HBM per device.

v0:
```python
import jax
import jax.numpy as jnp
from jax import lax
from jax.sharding import PartitionSpec as P


def merged(value, axis, join):
    pieces = jax.tree.map(lambda part: lax.all_gather(part, axis), value)
    head = jax.tree.map(lambda part: part[0], pieces)
    tail = jax.tree.map(lambda part: part[1:], pieces)
    subtotal, _ = lax.scan(lambda subtotal, share: (join(subtotal, share), None), head, tail)
    return subtotal


def combine_reads(first, second):
    top = jnp.maximum(first[0], second[0])
    scale_one = jnp.exp(first[0] - top)
    scale_two = jnp.exp(second[0] - top)
    total = first[1] * scale_one + second[1] * scale_two
    weighted = first[2] * scale_one[..., None] + second[2] * scale_two[..., None]
    return (top, total, weighted)


def partial_read(query, keys, values, gates, head_size):
    scores = jnp.einsum("bhe,bhse->bhs", query, keys, preferred_element_type=jnp.float32)
    scores = scores * head_size ** (-0.5) - gates
    top = jnp.max(scores, axis=-1)
    weights = jnp.exp(scores - top[..., None])
    total = jnp.sum(weights, axis=-1)
    weighted = jnp.einsum(
        "bhs,bhse->bhe", weights.astype(jnp.bfloat16), values, preferred_element_type=jnp.float32
    )
    return (top, total, weighted)


def local_project(tokens, key_weight, value_weight, head_size):
    width = tokens.shape[3]
    local_rows = tokens[:, 0]
    key_part = jnp.einsum(
        "btd,dhe->bhte",
        local_rows,
        key_weight.reshape(width, -1, head_size),
        preferred_element_type=jnp.float32,
    ).astype(jnp.bfloat16)
    value_part = jnp.einsum(
        "btd,dhe->bhte",
        local_rows,
        value_weight.reshape(width, -1, head_size),
        preferred_element_type=jnp.float32,
    ).astype(jnp.bfloat16)
    return (key_part, value_part)


def on_device(tokens, key_weight, value_weight, cum_gate, query):
    count = tokens.shape[0]
    head_size = query.shape[2]
    key_part = None
    value_part = None
    key_part, value_part = local_project(tokens, key_weight, value_weight, head_size)
    joined = jnp.concatenate([key_part, value_part], axis=-1)
    kv_cache = lax.all_to_all(joined, "sp", split_axis=1, concat_axis=2, tiled=True)
    gates = lax.all_to_all(cum_gate, "sp", split_axis=1, concat_axis=3, tiled=True)
    gate_cache = gates.reshape(count, gates.shape[1], gates.shape[3])
    parts = partial_read(
        query, kv_cache[..., :head_size], kv_cache[..., head_size:], gate_cache, head_size
    )
    top, total, weighted = merged(parts, "tp", combine_reads)
    read = (weighted / total[..., None]).astype(jnp.bfloat16)
    return (kv_cache, gate_cache, read)


def solution(mesh):
    placed = (P("gr", "tp", "sp", None), P(), P(), P("gr", None, "tp", "sp"), P("gr", "sp", None))
    return jax.shard_map(
        on_device,
        mesh=mesh,
        in_specs=placed,
        out_specs=(P("gr", "sp", "tp", None), P("gr", "sp", "tp"), P("gr", "sp", None)),
        check_vma=False,
    )
```

profile of v0, /device:TPU:0, one launch (start us, length us, event | category | flops | bytes accessed | tf_op | source)
XLA Modules:
  0.0 217.3 jit_solution(17733755915182481379)
XLA Ops:
  0.6 0.0 copy-start
  0.6 7.6 %all-to-all-start.1 = ((f32[1,32,1,768]{3,2,0,1:T(1,128)}), f32[1,32,1,768]{3,2,0,1:T(1,128)S(1)}, u32[]{:S(2)}, u32[]{:S(2)}) async-start(f32[1,32,1,768]{3,2,0,1:T(1,128)} %bitcast.77), calls=%async_computation.1 | async-start | bytes 196608 | tf_op jit(solution)/shard_map/all_to_all | solution.py:62
  8.2 12.3 %copy.23 = bf16[2048,2048]{0,1:T(8,128)(2,1)} copy(bf16[2048,2048]{1,0:T(8,128)(2,1)} %param.7) | data formatting | bytes 16777216 | tf_op args[2]
  20.5 12.4 %copy.22 = bf16[2048,2048]{0,1:T(8,128)(2,1)} copy(bf16[2048,2048]{1,0:T(8,128)(2,1)} %param.6) | data formatting | bytes 16777216 | tf_op args[1]
  32.9 0.0 copy-done
  32.9 9.3 %convert_bitcast_fusion = bf16[1,32,768,64]{2,3,1,0:T(8,128)(2,1)S(1)} fusion(bf16[2048,32,64]{0,2,1:T(8,128)(2,1)} %bitcast.68, bf16[1,1,768,2048]{3,2,1,0:T(8,128)(2,1)S(1)} %copy-done), kind=kOutput, calls=%fused_computation.9 | convolution fusion | flops 6444023808 | bytes 14680064 | tf_op jit(solution)/shard_map/btd,dhe->bhte/dot_general | solution.py:45
  42.2 6.9 %convert_bitcast_fusion.1 = bf16[1,32,768,64]{2,3,1,0:T(8,128)(2,1)S(1)} fusion(bf16[2048,32,64]{0,2,1:T(8,128)(2,1)S(1)} %bitcast.67, bf16[1,1,768,2048]{3,2,1,0:T(8,128)(2,1)S(1)} %copy-done), kind=kOutput, calls=%fused_computation.10 | convolution fusion | flops 6444023808 | bytes 14680064 | tf_op jit(solution)/shard_map/btd,dhe->bhte/dot_general | solution.py:39
  49.1 3.4 %maximum_bitcast_fusion = bf16[1,32,768,128]{2,3,0,1:T(8,128)(2,1)} fusion(bf16[1,32,768,64]{2,3,1,0:T(8,128)(2,1)S(1)} %convert_bitcast_fusion, bf16[1,32,768,64]{2,3,1,0:T(8,128)(2,1)S(1)} %convert_bitcast_fusion.1), kind=kLoop, calls=%fused_computation.4 | loop fusion | flops 12582912 | bytes 12582912 | tf_op jit(solution)/shard_map/concatenate | solution.py:60
  52.5 0.0 all-to-all-done.1
  52.5 6.1 %all-to-all-start = ((bf16[1,32,768,128]{2,3,0,1:T(8,128)(2,1)}), bf16[1,32,768,128]{2,3,0,1:T(8,128)(2,1)}, u32[]{:S(2)}, u32[]{:S(2)}) async-start(bf16[1,32,768,128]{2,3,0,1:T(8,128)(2,1)} %maximum_bitcast_fusion), calls=%async_computation | async-start | bytes 12582912 | tf_op jit(solution)/shard_map/all_to_all | solution.py:61
  58.6 0.6 dynamic-slice
  59.9 0.7 reshape.234
  60.6 135.7 %all-to-all-done = bf16[1,32,768,128]{2,3,0,1:T(8,128)(2,1)} async-done(((bf16[1,32,768,128]{2,3,0,1:T(8,128)(2,1)}), bf16[1,32,768,128]{2,3,0,1:T(8,128)(2,1)}, u32[]{:S(2)}, u32[]{:S(2)}) %all-to-all-start) | async-done | bytes 6291488 | tf_op jit(solution)/shard_map/all_to_all | solution.py:61
  196.3 8.6 %copy.25 = bf16[1,4,8,768,128]{4,3,2,1,0:T(8,128)(2,1)} copy(bf16[1,4,8,768,128]{3,4,1,2,0:T(8,128)(2,1)} %bitcast.11) | data formatting | bytes 12582912 | tf_op jit(solution)/shard_map/all_to_all | solution.py:61
  204.9 4.6 %fusion.1 = f32[4,1,6144]{2,1,0:T(1,128)S(1)} fusion(bf16[1,4,6144,128]{3,2,1,0:T(8,128)(2,1)} %bitcast.69, bf16[4,64,1]{1,0,2:T(4,128)(2,1)S(1)} %bitcast.79), kind=kOutput, calls=%fused_computation.3 | convolution fusion | flops 3145728 | bytes 6390272 | tf_op jit(solution)/shard_map/bhe,bhse->bhs/dot_general | solution.py:25
  209.5 0.2 fusion.22
  209.7 0.2 fusion.12
  210.0 1.9 fusion
  211.9 0.2 dynamic-update-slice
  212.1 0.2 dynamic-update-slice.1
  212.3 1.8 all-gather.3
  214.1 2.4 %all-reduce.2 = (f32[8]{0:T(128)S(1)}, f32[8]{0:T(128)S(1)}) all-reduce(f32[8]{0:T(128)S(1)} %dynamic-update-slice, f32[8]{0:T(128)S(1)} %dynamic-update-slice.1), channel_id=3, replica_groups=mesh['gr'=2,'sp'=8,'tp'=2] {'tp'}, use_global_device_ids=true, to_apply=%add | all-reduce | flops 16 | bytes 128
  216.6 0.1 fusion.21
  216.7 0.6 fusion.18
  (12 shorter events, 0.1 us)
Async XLA Ops:
  0.6 32.2 %copy-start = (bf16[1,1,768,2048]{3,2,1,0:T(8,128)(2,1)S(1)}, bf16[1,1,768,2048]{3,2,1,0:T(8,128)(2,1)}, u32[]{:S(2)}) copy-start(bf16[1,1,768,2048]{3,2,1,0:T(8,128)(2,1)} %param.5) | copy-start | bytes 9437188
  0.6 51.8 %all-to-all-start.1 = ((f32[1,32,1,768]{3,2,0,1:T(1,128)}), f32[1,32,1,768]{3,2,0,1:T(1,128)S(1)}, u32[]{:S(2)}, u32[]{:S(2)}) async-start(f32[1,32,1,768]{3,2,0,1:T(1,128)} %bitcast.77), calls=%async_computation.1 | async-start | bytes 196608 | tf_op jit(solution)/shard_map/all_to_all | solution.py:62
  32.9 9.3 %copy-start.1 = (bf16[2048,2048]{0,1:T(8,128)(2,1)S(1)}, bf16[2048,2048]{0,1:T(8,128)(2,1)}, u32[]{:S(2)}) copy-start(bf16[2048,2048]{0,1:T(8,128)(2,1)} %copy.22) | copy-start | bytes 25165828
  52.5 6.1 %copy-start.4 = (u32[32]{0:T(128)S(1)}, u32[32]{0:T(128)}, u32[]{:S(2)}) copy-start(u32[32]{0:T(128)} %constant.21) | copy-start | bytes 388
  52.5 143.8 %all-to-all-start = ((bf16[1,32,768,128]{2,3,0,1:T(8,128)(2,1)}), bf16[1,32,768,128]{2,3,0,1:T(8,128)(2,1)}, u32[]{:S(2)}, u32[]{:S(2)}) async-start(bf16[1,32,768,128]{2,3,0,1:T(8,128)(2,1)} %maximum_bitcast_fusion), calls=%async_computation | async-start | bytes 12582912 | tf_op jit(solution)/shard_map/all_to_all | solution.py:61
  196.3 8.6 %copy-start.3 = (bf16[1,4,64]{2,1,0:T(4,128)(2,1)S(1)}, bf16[1,4,64]{2,1,0:T(4,128)(2,1)}, u32[]{:S(2)}) copy-start(bf16[1,4,64]{2,1,0:T(4,128)(2,1)} %param.9) | copy-start | bytes 1540
  204.9 5.1 %copy-start.2 = (bf16[1,4,8,768,128]{4,3,2,1,0:T(8,128)(2,1)S(1)}, bf16[1,4,8,768,128]{4,3,2,1,0:T(8,128)(2,1)}, u32[]{:S(2)}) copy-start(bf16[1,4,8,768,128]{4,3,2,1,0:T(8,128)(2,1)} %copy.25) | copy-start | bytes 18874372
where the time goes:
time: 218 us; the launch traced here: 217 us
  waiting for transfers between devices  136 us (62%)
  local copies, waits for them, and re-layouts  35 us (16%)
  matrix products  22.8 us (10%)
  starting transfers between devices  13.7 us (6%)
  other arithmetic  4.53 us (2%)
  blocking collectives  4.27 us (2%)
    all_to_all x1, waiting for transfers between devices, on_device(): lax.all_to_all(joined, 'sp', split_axis=1, concat_axis=2, tiled=True)  136 us
    unnamed x18, local copies, waits for them, and re-layouts  25.7 us
    dot_general x1, matrix products, local_project(): jnp.einsum('btd,dhe->bhte', local_rows, value_weight.reshape(width, -1, h...  9.28 us
    all_to_all x1, local copies, waits for them, and re-layouts, on_device(): lax.all_to_all(joined, 'sp', split_axis=1, concat_axis=2, tiled=True)  8.63 us
    all_to_all x1, starting transfers between devices, on_device(): lax.all_to_all(cum_gate, 'sp', split_axis=1, concat_axis=3, tiled=True)  7.58 us
    dot_general x1, matrix products, local_project(): jnp.einsum('btd,dhe->bhte', local_rows, key_weight.reshape(width, -1, hea...  6.93 us
    all_to_all x1, starting transfers between devices, on_device(): lax.all_to_all(joined, 'sp', split_axis=1, concat_axis=2, tiled=True)  6.12 us
    dot_general x1, matrix products, partial_read(): jnp.einsum('bhe,bhse->bhs', query, keys, preferred_element_type=jnp.float32)  4.64 us
  transfers between devices with their start and end apart: 2, of which 1 were waited for; matrix products, arithmetic and copies ran while one was open for 21% of the time, Pallas kernels for 0%

commit v1 on v0

--- a/solution.py
+++ b/solution.py
@@ -58,7 +58,9 @@
     value_part = None
     key_part, value_part = local_project(tokens, key_weight, value_weight, head_size)
     joined = jnp.concatenate([key_part, value_part], axis=-1)
-    kv_cache = lax.all_to_all(joined, "sp", split_axis=1, concat_axis=2, tiled=True)
+    kv_cache = jnp.concatenate(
+        lax.all_to_all(jnp.stack(jnp.split(joined, lax.axis_size("sp"), 1)), "sp", 0, 0), 2
+    )
     gates = lax.all_to_all(cum_gate, "sp", split_axis=1, concat_axis=3, tiled=True)
     gate_cache = gates.reshape(count, gates.shape[1], gates.shape[3])
     parts = partial_read(

time: 218 us -> 222 us (1.018)
  other arithmetic: 4.53 us -> 8.62 us
    all_to_all x1 -> x0, local copies, waits for them, and re-layouts: 8.63 us -> none  [on_device(): lax.all_to_all(joined, 'sp', split_axis=1, concat_axis=2, tiled=True)]
    reshape x0 -> x1, local copies, waits for them, and re-layouts: none -> 8.63 us  [on_device(): jnp.concatenate(lax.all_to_all(jnp.stack(jnp.split(joined, lax.axis_size(...]
    unnamed x0 -> x7, other arithmetic: none -> 6.52 us
    concatenate x1 -> x0, other arithmetic: 3.36 us -> none  [on_device(): joined = jnp.concatenate([key_part, value_part], axis=-1)]
  transfers between devices with their start and end apart: 2 -> 2, of which waited for: 1 -> 1; matrix products, arithmetic and copies ran while one was open for 21% -> 22% of each run, Pallas kernels for 0% -> 0%
where the time goes in v1:
time: 222 us; the launch traced here: 221 us
  waiting for transfers between devices  136 us (61%)
  local copies, waits for them, and re-layouts  35 us (16%)
  matrix products  22.8 us (10%)
  starting transfers between devices  13.7 us (6%)
  other arithmetic  8.62 us (4%)
  blocking collectives  4.27 us (2%)
    all_to_all x1, waiting for transfers between devices, on_device(): lax.all_to_all(jnp.stack(jnp.split(joined, lax.axis_size('sp'), 1)), 'sp'...  136 us
    unnamed x18, local copies, waits for them, and re-layouts  25.7 us
    dot_general x1, matrix products, local_project(): jnp.einsum('btd,dhe->bhte', local_rows, value_weight.reshape(width, -1, h...  9.28 us
    reshape x1, local copies, waits for them, and re-layouts, on_device(): jnp.concatenate(lax.all_to_all(jnp.stack(jnp.split(joined, lax.axis_size(...  8.63 us
    all_to_all x1, starting transfers between devices, on_device(): lax.all_to_all(cum_gate, 'sp', split_axis=1, concat_axis=3, tiled=True)  7.58 us
    dot_general x1, matrix products, local_project(): jnp.einsum('btd,dhe->bhte', local_rows, key_weight.reshape(width, -1, hea...  6.93 us
    unnamed x7, other arithmetic  6.52 us
    all_to_all x1, starting transfers between devices, on_device(): lax.all_to_all(jnp.stack(jnp.split(joined, lax.axis_size('sp'), 1)), 'sp'...  6.12 us
  transfers between devices with their start and end apart: 2, of which 1 were waited for; matrix products, arithmetic and copies ran while one was open for 22% of the time, Pallas kernels for 0%

profile of v1, /device:TPU:0, one launch (start us, length us, event | category | flops | bytes accessed | tf_op | source)
XLA Modules:
  0.0 221.4 jit_solution(11147928914449794682)
XLA Ops:
  0.6 7.6 %all-to-all-start.1 = ((f32[1,32,1,768]{3,2,0,1:T(1,128)}), f32[1,32,1,768]{3,2,0,1:T(1,128)S(1)}, u32[]{:S(2)}, u32[]{:S(2)}) async-start(f32[1,32,1,768]{3,2,0,1:T(1,128)} %bitcast.91), calls=%async_computation.1 | async-start | bytes 196608 | tf_op jit(solution)/shard_map/all_to_all | solution.py:64
  8.2 12.3 %copy.21 = bf16[2048,2048]{0,1:T(8,128)(2,1)} copy(bf16[2048,2048]{1,0:T(8,128)(2,1)} %param.7) | data formatting | bytes 16777216 | tf_op args[2]
  20.5 12.4 %copy.20 = bf16[2048,2048]{0,1:T(8,128)(2,1)} copy(bf16[2048,2048]{1,0:T(8,128)(2,1)} %param.6) | data formatting | bytes 16777216 | tf_op args[1]
  32.9 9.3 %convert_bitcast_fusion = bf16[1,32,768,64]{2,3,1,0:T(8,128)(2,1)S(1)} fusion(bf16[2048,32,64]{0,2,1:T(8,128)(2,1)} %bitcast.82, bf16[1,1,768,2048]{3,2,1,0:T(8,128)(2,1)S(1)} %copy-done), kind=kOutput, calls=%fused_computation.22 | convolution fusion | flops 6444023808 | bytes 14680064 | tf_op jit(solution)/shard_map/btd,dhe->bhte/dot_general | solution.py:45
  42.2 6.9 %convert_bitcast_fusion.1 = bf16[1,32,768,64]{2,3,1,0:T(8,128)(2,1)S(1)} fusion(bf16[2048,32,64]{0,2,1:T(8,128)(2,1)S(1)} %bitcast.81, bf16[1,1,768,2048]{3,2,1,0:T(8,128)(2,1)S(1)} %copy-done), kind=kOutput, calls=%fused_computation.23 | convolution fusion | flops 6444023808 | bytes 14680064 | tf_op jit(solution)/shard_map/btd,dhe->bhte/dot_general | solution.py:39
  49.1 0.9 bitcast_dynamic-update-slice_fusion.6
  50.0 0.9 bitcast_dynamic-update-slice_fusion.5
  51.0 0.9 bitcast_dynamic-update-slice_fusion.4
  51.9 0.9 bitcast_dynamic-update-slice_fusion.3
  52.8 0.9 bitcast_dynamic-update-slice_fusion.2
  53.8 0.9 bitcast_dynamic-update-slice_fusion.1
  54.7 0.9 bitcast_dynamic-update-slice_fusion
  55.6 0.9 fusion.18
  56.6 6.1 %all-to-all-start = ((bf16[8,1,4,768,128]{3,4,2,1,0:T(8,128)(2,1)}), bf16[8,1,4,768,128]{3,4,2,1,0:T(8,128)(2,1)}, u32[]{:S(2)}, u32[]{:S(2)}) async-start(bf16[8,1,4,768,128]{3,4,2,1,0:T(8,128)(2,1)} %fusion.18), calls=%async_computation | async-start | bytes 12582912 | tf_op jit(solution)/shard_map/all_to_all | solution.py:62
  62.7 0.6 dynamic-slice
  64.0 0.7 reshape.242
  64.7 135.7 %all-to-all-done = bf16[8,1,4,768,128]{3,4,2,1,0:T(8,128)(2,1)} async-done(((bf16[8,1,4,768,128]{3,4,2,1,0:T(8,128)(2,1)}), bf16[8,1,4,768,128]{3,4,2,1,0:T(8,128)(2,1)}, u32[]{:S(2)}, u32[]{:S(2)}) %all-to-all-start) | async-done | bytes 6291488 | tf_op jit(solution)/shard_map/all_to_all | solution.py:62
  200.3 8.6 %copy.22 = bf16[1,4,8,768,128]{4,3,2,1,0:T(8,128)(2,1)} copy(bf16[1,4,8,768,128]{3,4,1,0,2:T(8,128)(2,1)} %bitcast.17) | data formatting | bytes 12582912 | tf_op jit(solution)/shard_map/reshape | solution.py:61
  209.0 4.6 %fusion.1 = f32[4,1,6144]{2,1,0:T(1,128)S(1)} fusion(bf16[1,4,6144,128]{3,2,1,0:T(8,128)(2,1)} %bitcast.83, bf16[4,64,1]{1,0,2:T(4,128)(2,1)S(1)} %bitcast.93), kind=kOutput, calls=%fused_computation.17 | convolution fusion | flops 3145728 | bytes 6390272 | tf_op jit(solution)/shard_map/bhe,bhse->bhs/dot_general | solution.py:25
  213.8 0.2 fusion.21
  214.1 1.9 fusion
  216.4 1.8 all-gather.3
  218.2 2.4 %all-reduce.2 = (f32[8]{0:T(128)S(1)}, f32[8]{0:T(128)S(1)}) all-reduce(f32[8]{0:T(128)S(1)} %dynamic-update-slice, f32[8]{0:T(128)S(1)} %dynamic-update-slice.1), channel_id=3, replica_groups=mesh['gr'=2,'sp'=8,'tp'=2] {'tp'}, use_global_device_ids=true, to_apply=%add | all-reduce | flops 16 | bytes 128
  220.8 0.6 fusion.27
  (19 shorter events, 0.8 us)
Async XLA Ops:
  0.6 32.2 %copy-start = (bf16[1,1,768,2048]{3,2,1,0:T(8,128)(2,1)S(1)}, bf16[1,1,768,2048]{3,2,1,0:T(8,128)(2,1)}, u32[]{:S(2)}) copy-start(bf16[1,1,768,2048]{3,2,1,0:T(8,128)(2,1)} %param.5) | copy-start | bytes 9437188
  0.6 55.9 %all-to-all-start.1 = ((f32[1,32,1,768]{3,2,0,1:T(1,128)}), f32[1,32,1,768]{3,2,0,1:T(1,128)S(1)}, u32[]{:S(2)}, u32[]{:S(2)}) async-start(f32[1,32,1,768]{3,2,0,1:T(1,128)} %bitcast.91), calls=%async_computation.1 | async-start | bytes 196608 | tf_op jit(solution)/shard_map/all_to_all | solution.py:64
  32.9 9.3 %copy-start.1 = (bf16[2048,2048]{0,1:T(8,128)(2,1)S(1)}, bf16[2048,2048]{0,1:T(8,128)(2,1)}, u32[]{:S(2)}) copy-start(bf16[2048,2048]{0,1:T(8,128)(2,1)} %copy.20) | copy-start | bytes 25165828
  56.6 6.1 %copy-start.4 = (u32[32]{0:T(128)S(1)}, u32[32]{0:T(128)}, u32[]{:S(2)}) copy-start(u32[32]{0:T(128)} %constant.21) | copy-start | bytes 388
  56.6 143.8 %all-to-all-start = ((bf16[8,1,4,768,128]{3,4,2,1,0:T(8,128)(2,1)}), bf16[8,1,4,768,128]{3,4,2,1,0:T(8,128)(2,1)}, u32[]{:S(2)}, u32[]{:S(2)}) async-start(bf16[8,1,4,768,128]{3,4,2,1,0:T(8,128)(2,1)} %fusion.18), calls=%async_computation | async-start | bytes 12582912 | tf_op jit(solution)/shard_map/all_to_all | solution.py:62
  200.3 8.6 %copy-start.3 = (bf16[1,4,64]{2,1,0:T(4,128)(2,1)S(1)}, bf16[1,4,64]{2,1,0:T(4,128)(2,1)}, u32[]{:S(2)}) copy-start(bf16[1,4,64]{2,1,0:T(4,128)(2,1)} %param.9) | copy-start | bytes 1540
  209.0 5.1 %copy-start.2 = (bf16[1,4,8,768,128]{4,3,2,1,0:T(8,128)(2,1)S(1)}, bf16[1,4,8,768,128]{4,3,2,1,0:T(8,128)(2,1)}, u32[]{:S(2)}) copy-start(bf16[1,4,8,768,128]{4,3,2,1,0:T(8,128)(2,1)} %copy.22) | copy-start | bytes 18874372
